TPU v7x, 256 devices: a whole 4x4x8 slice. The times are simulated.
256 devices in a mesh: ep: 16 (over y, x), tp: 16 (over z, core).
Axes of the slice: x: 4, y: 4, z: 8, core: 2. Of those that a mesh axis runs over, the one named last changes fastest.
Arguments:
- pool_input: bfloat16 [32768, 1024], P('ep', 'tp'), may hold values from -6 to 6
- pool_gain: float32 [1024], P('tp'), may hold values from 0.1 to 1.9
- mix_weight: bfloat16 [1024, 2048], P('tp'), may hold values from -0.1875 to 0.1875
- moe_input: bfloat16 [65536, 2048], P(('ep', 'tp')), may hold values from -6 to 6
- moe_gain: float32 [2048], replicated, may hold values from 0.1 to 1.9
- expert_ids: int32 [65536, 2], P(('ep', 'tp')), may hold values from 0 to 15, as said below
- route_weight: float32 [65536, 2], P(('ep', 'tp')), may hold values from 0.2 to 1
- gate_weight: bfloat16 [16, 2048, 1024], P('ep', None, 'tp'), may hold values from -0.125 to 0.125
- up_weight: bfloat16 [16, 2048, 1024], P('ep', None, 'tp'), may hold values from -0.125 to 0.125
- down_weight: bfloat16 [16, 2048, 1024], P('ep', None, 'tp'), may hold values from -0.1875 to 0.1875
Outputs:
- mixed_out: bfloat16 [32768, 2048], P(('ep', 'tp'))
- moe_out: bfloat16 [65536, 2048], P(('ep', 'tp'))
Inputs may be any that keep to these rules, and one draw needn't show every extreme that they name: `expert_ids`: each row names 2 different experts of one group of 4 consecutive experts. In each aligned block of 256 rows (the rows of one device) no expert is named by more than 48 rows, and some expert is named by exactly 48 rows.
All inputs are finite; a program needn't handle non-finite values.
Results may differ from a plain program's by a relative error of at most 0.012.
Values may be sent and summed in bfloat16 or wider, within the bound.
A program may use at most 128 MiB of HBM per device.

v0:
```python
import jax
import jax.numpy as jnp
from jax import lax
from jax.sharding import PartitionSpec as P

GROUP_CH = 256
EXPERTS = 16
TOP = 2
CAP = 48
eps_norm = 1e-06


def from_behind(shard, axis, by):
    peers = lax.axis_size(axis)
    pairs = [(i, i + by) for i in range(peers) if 0 <= i + by < peers]
    return lax.ppermute(shard, axis, pairs)


def gather_turned(arrays, axis, dims):
    turned = [jnp.moveaxis(a, dim, 0) for a, dim in zip(arrays, dims)]
    both = jnp.concatenate([t.reshape(len(t), -1) for t in turned], axis=1)
    result, at, gathered = (lax.all_gather(both, axis, axis=0, tiled=True), 0, [])
    for t, dim in zip(turned, dims):
        section = result[:, at : at + t[0].size].reshape(-1, *t.shape[1:])
        gathered.append(jnp.moveaxis(section, 0, dim))
        at += t[0].size
    return tuple(gathered)


def in_blocks(shard, dim, peers):
    before, after = (shard.shape[:dim], shard.shape[dim + 1 :])
    return jnp.moveaxis(shard.reshape(*before, peers, -1, *after), dim, 0)


def cut_rows(length, count):
    unit = 8 if length >= 8 * count else 1
    return [length // unit * k // count * unit for k in range(1, count)]


def joined_along(tiles, dim):
    tiles = jnp.moveaxis(tiles, 0, dim)
    dims = tiles.shape
    return tiles.reshape(*dims[:dim], dims[dim] * dims[dim + 1], *dims[dim + 2 :])


def exchange_in_pieces(shard, axis, pieces, split_dim, concat_dim):
    tiles = in_blocks(shard, split_dim, lax.axis_size(axis))
    widest = max(range(1, max(2, tiles.ndim - 1)), key=lambda d: tiles.shape[d])
    gathered = []
    for section in jnp.split(tiles, cut_rows(tiles.shape[widest], pieces), axis=widest):
        if section.size:
            gathered.append(lax.all_to_all(section, axis, split_axis=0, concat_axis=0, tiled=True))
    return joined_along(jnp.concatenate(gathered, axis=widest), concat_dim)


def window_sums(extended, row_count):
    level_sum = extended
    stride = 1
    outputs = []
    for doubling in range(4):
        level_sum = level_sum[stride:] + level_sum[:-stride]
        stride = stride * 2
        outputs.append(level_sum[level_sum.shape[0] - row_count :])
    return outputs


def pool_mixer(pool_input, pool_gain):
    row_count, channels = pool_input.shape
    carried = from_behind(pool_input[row_count - 15 :], "ep", 1)
    extended = jnp.concatenate([carried, pool_input], axis=0).astype(jnp.float32)
    window_list = window_sums(extended, row_count)
    channel_ids = lax.axis_index("tp") * channels + lax.iota(jnp.int32, channels)
    group_ids = channel_ids // GROUP_CH
    position = lax.axis_index("ep") * row_count + lax.iota(jnp.int32, row_count)
    summed = jnp.zeros((row_count, channels), jnp.float32)
    widths = jnp.zeros((channels,), jnp.int32)
    for index_group in range(4):
        inside = group_ids == index_group
        summed = jnp.where(inside[None, :], window_list[index_group], summed)
        widths = jnp.where(inside, 2 ** (index_group + 1), widths)
    counted = jnp.minimum(position[:, None] + 1, widths[None, :]).astype(jnp.float32)
    values = extended[15:]
    return ((summed / counted - values) * pool_gain).astype(jnp.bfloat16)


def route_slots(expert_ids):
    flat_ids = expert_ids.reshape(-1)
    marked = (flat_ids[:, None] == lax.iota(jnp.int32, EXPERTS)[None, :]).astype(jnp.int32)
    before_count = jnp.cumsum(marked, axis=0) - marked
    ranked = jnp.sum(before_count * marked, axis=1)
    return (flat_ids * CAP + ranked).reshape(expert_ids.shape)


def body(
    pool_input,
    pool_gain,
    mix_weight,
    moe_input,
    moe_gain,
    expert_ids,
    route_weight,
    gate_weight,
    up_weight,
    down_weight,
):
    pooled = pool_mixer(pool_input, pool_gain)
    mixed_sum = lax.psum_scatter(
        jnp.dot(pooled, mix_weight, preferred_element_type=jnp.float32).astype(jnp.bfloat16),
        "tp",
        scatter_dimension=0,
        tiled=True,
    )
    inputs = moe_input.astype(jnp.float32)
    scale_rows = lax.rsqrt(jnp.mean(inputs * inputs, axis=-1, keepdims=True) + eps_norm)
    normed = (inputs * scale_rows * moe_gain).astype(jnp.bfloat16)
    slots = route_slots(expert_ids)
    slot_index = lax.iota(jnp.int32, EXPERTS * CAP)
    placing = (
        (slot_index[:, None] == slots[None, :, 0]) | (slot_index[:, None] == slots[None, :, 1])
    ).astype(jnp.bfloat16)
    outgoing = jnp.dot(placing, normed, preferred_element_type=jnp.float32).astype(jnp.bfloat16)
    outgoing = outgoing.reshape(EXPERTS, CAP, normed.shape[1])
    arrived = lax.all_to_all(outgoing, "ep", split_axis=0, concat_axis=1, tiled=True)
    gate_piece, up_piece, down_piece = gather_turned(
        (gate_weight, up_weight, down_weight), "tp", (2, 2, 2)
    )
    gate_part = jnp.einsum("erd,edf->erf", arrived, gate_piece, preferred_element_type=jnp.float32)
    upward = jnp.einsum("erd,edf->erf", arrived, up_piece, preferred_element_type=jnp.float32)
    hidden = (jax.nn.silu(gate_part) * upward).astype(jnp.bfloat16)
    expert_sum = jnp.einsum("erf,edf->erd", hidden, down_piece, preferred_element_type=jnp.float32)
    expert_rows = expert_sum.astype(jnp.bfloat16)
    returned = exchange_in_pieces(expert_rows, "ep", 2, 1, 0)
    returned_rows = returned.reshape(EXPERTS * CAP, returned.shape[2])
    combined = jnp.zeros((normed.shape[0], normed.shape[1]), jnp.float32)
    for route_index in range(TOP):
        picking = (slots[:, route_index][:, None] == slot_index[None, :]).astype(jnp.bfloat16)
        chosen_rows = jnp.dot(picking, returned_rows, preferred_element_type=jnp.float32)
        combined = combined + route_weight[:, route_index : route_index + 1] * chosen_rows
    moe_out = combined.astype(jnp.bfloat16)
    return (mixed_sum, moe_out)


def solution(mesh):
    return jax.shard_map(
        body,
        mesh=mesh,
        in_specs=(
            P("ep", "tp"),
            P("tp"),
            P("tp", None),
            P(("ep", "tp"), None),
            P(),
            P(("ep", "tp"), None),
            P(("ep", "tp"), None),
            P("ep", None, "tp"),
            P("ep", None, "tp"),
            P("ep", None, "tp"),
        ),
        out_specs=(P(("ep", "tp"), None), P(("ep", "tp"), None)),
        check_vma=False,
    )
```

profile of v0, /device:TPU:24, one launch (start us, length us, event | category | flops | bytes accessed | tf_op | source)
XLA Modules:
  0.0 169.4 jit_solution(2128738845076339087)
XLA Ops:
  7.2 2.1 %pad_maximum_fusion.1 = bf16[64,6144]{1,0:T(8,128)(2,1)} fusion(bf16[64,2048]{1,0:T(8,128)(2,1)} %bitcast.76, bf16[64,2048]{1,0:T(8,128)(2,1)} %bitcast.77, bf16[64,2048]{1,0:T(8,128)(2,1)} %bitcast.78), kind=kLoop, calls=%fused_computation.22 | loop fusion | flops 2359296 | bytes 1572864 | tf_op jit(solution)/shard_map/concatenate | solution.py:21
  9.4 0.8 slice.66
  10.2 3.4 %collective-permute-start = (bf16[15,64]{0,1:T(8,128)(2,1)S(1)}, bf16[15,64]{0,1:T(8,128)(2,1)S(1)}, u32[]{:S(2)}, u32[]{:S(2)}) collective-permute-start(bf16[15,64]{0,1:T(8,128)(2,1)S(1)} %slice.66), channel_id=1, source_target_pairs={{0,16},{16,32},{32,48},{48,64},{64,80},{80,96},{96,112},{112,128},... | collective-permute-start | bytes 5768 | tf_op jit(solution)/shard_map/ppermute | solution.py:16
  13.7 4.3 %collective-permute-done = bf16[15,64]{0,1:T(8,128)(2,1)S(1)} collective-permute-done((bf16[15,64]{0,1:T(8,128)(2,1)S(1)}, bf16[15,64]{0,1:T(8,128)(2,1)S(1)}, u32[]{:S(2)}, u32[]{:S(2)}) %collective-permute-start) | collective-permute-done | bytes 1952 | tf_op jit(solution)/shard_map/ppermute | solution.py:16
  17.9 1.1 maximum_convert_fusion
  19.7 6.5 %convolution_convert_fusion = bf16[2048,2048]{1,0:T(8,128)(2,1)} fusion(bf16[64,2048]{1,0:T(8,128)(2,1)S(1)} %copy-done, f32[2063,64]{0,1:T(8,128)S(1)} %maximum_convert_fusion, f32[2062,64]{0,1:T(8,128)S(1)} %slice_add_fusion.2, f32[2060,64]{0,1:T(8,128)S(1)} %slice_add_fusion.1, f32[2056,64]{0,1:T(8,128)S(1)} %slice_add_fusion, f32[64]{0:T(128)S(1)} %copy-done.4, ...), kind=kOutput, calls=%fused_computation | convolution fusion | flops 542507008 | bytes 11283456 | tf_op jit(solution)/shard_map/dot_general | solution.py:108
  26.2 0.7 copy-done.3
  27.3 1.2 reduce-window.6
  29.0 0.3 fusion.6
  29.4 1.1 convolution_convert_fusion.1
  30.5 41.2 %all_to_all.19 = bf16[16,48,2048]{2,1,0:T(8,128)(2,1)S(1)} all-to-all(bf16[16,48,2048]{2,1,0:T(8,128)(2,1)S(1)} %bitcast.72), channel_id=1, replica_groups=mesh['ep'=16,'tp'=16] {'ep'}, dimensions={0} | all-to-all | bytes 6291456 | tf_op jit(solution)/shard_map/all_to_all | solution.py:123
  71.7 17.0 %all-gather.2.cloned.1.call-done = bf16[1024,6144]{1,0:T(8,128)(2,1)} async-done(((bf16[64,6144]{1,0:T(8,128)(2,1)}), bf16[1024,6144]{1,0:T(8,128)(2,1)}) %all-gather.2.cloned.1.call-update) | async-done | bytes 12582928 | tf_op jit(solution)/shard_map/all_gather | solution.py:22
  88.7 5.4 %fusion.1 = f32[768,1024]{1,0:T(8,128)S(1)} fusion(bf16[768,2048]{1,0:T(8,128)(2,1)S(1)} %bitcast.73, bf16[1024,6144]{1,0:T(8,128)(2,1)} %all-gather.2.cloned.1.call-done), kind=kOutput, calls=%fused_computation.4 | convolution fusion | flops 3221225472 | bytes 10485760 | tf_op jit(solution)/shard_map/erd,edf->erf/dot_general | solution.py:128
  94.1 0.4 copy-done.6
  94.6 3.9 %multiply_convert_fusion = bf16[768,1024]{1,0:T(8,128)(2,1)S(1)} fusion(f32[768,1024]{1,0:T(8,128)S(1)} %fusion.1, bf16[768,2048]{1,0:T(8,128)(2,1)S(1)} %bitcast.74, bf16[1024,6144]{1,0:T(8,128)(2,1)S(1)} %copy-done.6), kind=kOutput, calls=%fused_computation.10 | convolution fusion | flops 3225944064 | bytes 12058624 | tf_op jit(solution)/shard_map/erd,edf->erf/dot_general | solution.py:127
  98.4 3.6 %fusion.3 = bf16[768,2048]{1,0:T(8,128)(2,1)S(1)} fusion(bf16[768,1024]{1,0:T(8,128)(2,1)S(1)} %multiply_convert_fusion, bf16[1024,6144]{1,0:T(8,128)(2,1)S(1)} %copy-done.6), kind=kOutput, calls=%fused_computation.7 | convolution fusion | flops 3222798336 | bytes 8912896 | tf_op jit(solution)/shard_map/erf,edf->erd/dot_general | solution.py:130
  102.1 1.4 fusion.38
  103.5 28.0 %all_to_all.20 = bf16[16,1,24,2048]{3,2,1,0:T(8,128)(2,1)S(1)} all-to-all(bf16[16,1,24,2048]{3,2,1,0:T(8,128)(2,1)S(1)} %get-tuple-element.2), channel_id=1, replica_groups=mesh['ep'=16,'tp'=16] {'ep'}, dimensions={0} | all-to-all | bytes 3145728 | tf_op jit(solution)/shard_map/all_to_all | solution.py:52
  131.5 6.0 %all-to-all-start.2 = ((bf16[16,1,24,2048]{3,2,1,0:T(8,128)(2,1)}), bf16[16,1,24,2048]{3,2,1,0:T(8,128)(2,1)S(1)}, u32[]{:S(2)}, u32[]{:S(2)}) async-start(bf16[16,1,24,2048]{3,2,1,0:T(8,128)(2,1)} %get-tuple-element.3), calls=%async_computation.3 | async-start | bytes 3145728 | tf_op jit(solution)/shard_map/all_to_all | solution.py:52
  137.5 21.1 %all-to-all-done.2 = bf16[16,1,24,2048]{3,2,1,0:T(8,128)(2,1)S(1)} async-done(((bf16[16,1,24,2048]{3,2,1,0:T(8,128)(2,1)}), bf16[16,1,24,2048]{3,2,1,0:T(8,128)(2,1)S(1)}, u32[]{:S(2)}, u32[]{:S(2)}) %all-to-all-start.2) | async-done | bytes 1572896 | tf_op jit(solution)/shard_map/all_to_all | solution.py:52
  158.5 0.4 pad_maximum_fusion
  158.9 1.1 convolution_multiply_fusion.1
  160.0 2.1 %fusion.5 = bf16[256,2048]{1,0:T(8,128)(2,1)} fusion(f32[256,2048]{1,0:T(8,128)S(1)} %convolution_multiply_fusion.1, bf16[768,2048]{1,0:T(8,128)(2,1)S(1)} %bitcast.71, f32[256]{0:T(256)S(1)} %bitcast.81, s32[256]{0:T(256)S(1)} %bitcast.80), kind=kOutput, calls=%fused_computation.16 | convolution fusion | flops 807075840 | bytes 6293504 | tf_op jit(solution)/shard_map/dot_general | solution.py:137
  162.1 0.4 reduce-scatter.2.cloned.1.call-done
  (37 shorter events, 1.8 us)
Async XLA Ops:
  7.2 12.5 %copy-start = (bf16[64,2048]{1,0:T(8,128)(2,1)S(1)}, bf16[64,2048]{1,0:T(8,128)(2,1)}, u32[]{:S(2)}) copy-start(bf16[64,2048]{1,0:T(8,128)(2,1)} %param.12) | copy-start | bytes 786436
  7.2 81.5 %all-gather.2.cloned.1.call-start = ((), (), s32[]{:S(2)}) async-start(), calls=%async_computation.5 | async-start | bytes 13369344 | tf_op jit(solution)/shard_map/all_gather | solution.py:22
  9.3 10.4 %copy-start.4 = (f32[64]{0:T(128)S(1)}, f32[64]{0:T(128)}, u32[]{:S(2)}) copy-start(f32[64]{0:T(128)} %param.11) | copy-start | bytes 772
  9.3 153.2 %reduce-scatter.2.cloned.1.call-start = ((), (), s32[]{:S(2)}) async-start(), calls=%async_computation.4 | async-start | bytes 8912896 | tf_op jit(solution)/shard_map/reduce_scatter | solution.py:107
  10.2 7.7 %collective-permute-start = (bf16[15,64]{0,1:T(8,128)(2,1)S(1)}, bf16[15,64]{0,1:T(8,128)(2,1)S(1)}, u32[]{:S(2)}, u32[]{:S(2)}) collective-permute-start(bf16[15,64]{0,1:T(8,128)(2,1)S(1)} %slice.66), channel_id=1, source_target_pairs={{0,16},{16,32},{32,48},{48,64},{64,80},{80,96},{96,112},{112,128},... | collective-permute-start | bytes 5768 | tf_op jit(solution)/shard_map/ppermute | solution.py:16
  26.2 0.7 copy-start.3
  26.2 2.9 %copy-start.1 = (bf16[256,2048]{1,0:T(8,128)(2,1)S(1)}, bf16[256,2048]{1,0:T(8,128)(2,1)}, u32[]{:S(2)}) copy-start(bf16[256,2048]{1,0:T(8,128)(2,1)} %param.13) | copy-start | bytes 3145732
  26.2 3.2 %copy-start.2 = (f32[2048]{0:T(1024)S(1)}, f32[2048]{0:T(1024)}, u32[]{:S(2)}) copy-start(f32[2048]{0:T(1024)} %param.14) | copy-start | bytes 24580
  88.7 5.8 %copy-start.6 = (bf16[1024,6144]{1,0:T(8,128)(2,1)S(1)}, bf16[1024,6144]{1,0:T(8,128)(2,1)}, u32[]{:S(2)}) copy-start(bf16[1024,6144]{1,0:T(8,128)(2,1)} %all-gather.2.cloned.1.call-done) | copy-start | bytes 37748740
  103.5 34.0 %copy-start.5 = (f32[256,2]{0,1:T(2,128)S(1)}, f32[256,2]{0,1:T(2,128)}, u32[]{:S(2)}) copy-start(f32[256,2]{0,1:T(2,128)} %param.16) | copy-start | bytes 6148
  131.5 27.0 %all-to-all-start.2 = ((bf16[16,1,24,2048]{3,2,1,0:T(8,128)(2,1)}), bf16[16,1,24,2048]{3,2,1,0:T(8,128)(2,1)S(1)}, u32[]{:S(2)}, u32[]{:S(2)}) async-start(bf16[16,1,24,2048]{3,2,1,0:T(8,128)(2,1)} %get-tuple-element.3), calls=%async_computation.3 | async-start | bytes 3145728 | tf_op jit(solution)/shard_map/all_to_all | solution.py:52
Sparse Core Ops, SparseCore 0:
  10.4 78.2 all-gather.1
  91.8 70.6 reduce-scatter.1
where the time goes:
time: 170 us; the launch traced here: 169 us
  blocking collectives  69.2 us (41%)
  waiting for transfers between devices  42.8 us (25%)
  matrix products  23.8 us (14%)
  between operations  14.3 us (8%)
  starting transfers between devices  9.42 us (6%)
  other arithmetic  5.79 us (3%)
  local copies, waits for them, and re-layouts  4.17 us (2%)
    all_to_all x1, blocking collectives, body(): lax.all_to_all(outgoing, 'ep', split_axis=0, concat_axis=1, tiled=True)  41.2 us
    all_to_all x1, blocking collectives, exchange_in_pieces(): lax.all_to_all(section, axis, split_axis=0, concat_axis=0, tiled=True)  28 us
    all_to_all x1, waiting for transfers between devices, exchange_in_pieces(): lax.all_to_all(section, axis, split_axis=0, concat_axis=0, tiled=True)  21.1 us
    all_gather x1, waiting for transfers between devices, gather_turned(): lax.all_gather(both, axis, axis=0, tiled=True)  17 us
    dot_general x1, matrix products, body(): jnp.dot(pooled, mix_weight, preferred_element_type=jnp.float32)  6.48 us
    all_to_all x1, starting transfers between devices, exchange_in_pieces(): lax.all_to_all(section, axis, split_axis=0, concat_axis=0, tiled=True)  5.95 us
    dot_general x1, matrix products, body(): jnp.einsum('erd,edf->erf', arrived, up_piece, preferred_element_type=jnp....  5.42 us
    ppermute x1, waiting for transfers between devices, from_behind(): return lax.ppermute(shard, axis, pairs)  4.26 us
  transfers between devices with their start and end apart: 4, of which 4 were waited for; matrix products, arithmetic and copies ran while one was open for 18% of the time, Pallas kernels for 0%

commit v1 on v0

--- a/solution.py
+++ b/solution.py
@@ -1,3 +1,4 @@
+import functools
 import jax
 import jax.numpy as jnp
 from jax import lax
@@ -8,6 +9,15 @@
 TOP = 2
 CAP = 48
 eps_norm = 1e-06
+
+
+def time_desk(xx, dimension_no, ndim_at):
+    taken_in = jnp.stack(jnp.split(xx, lax.axis_size("ep"), axis=dimension_no))
+    mid_arr = lax.all_to_all(taken_in, "ep", 0, 0)
+    return jnp.concatenate(mid_arr, axis=ndim_at)
+
+
+work_hubs = functools.partial(time_desk, dimension_no=0, ndim_at=1)
 
 
 def from_behind(shard, axis, by):
@@ -120,7 +130,7 @@
     ).astype(jnp.bfloat16)
     outgoing = jnp.dot(placing, normed, preferred_element_type=jnp.float32).astype(jnp.bfloat16)
     outgoing = outgoing.reshape(EXPERTS, CAP, normed.shape[1])
-    arrived = lax.all_to_all(outgoing, "ep", split_axis=0, concat_axis=1, tiled=True)
+    arrived = work_hubs(outgoing)
     gate_piece, up_piece, down_piece = gather_turned(
         (gate_weight, up_weight, down_weight), "tp", (2, 2, 2)
     )

time: 170 us -> 170 us (level)
  waiting for transfers between devices: 42.8 us -> 28.5 us
  local copies, waits for them, and re-layouts: 4.17 us -> 15.4 us
  blocking collectives: 69.2 us -> 72 us
    unnamed x15 -> x32, local copies, waits for them, and re-layouts: 1.23 us -> 11.7 us
    all_gather x1, waiting for transfers between devices: 17 us -> 6.94 us  [gather_turned(): lax.all_gather(both, axis, axis=0, tiled=True)]
    ppermute x1, waiting for transfers between devices: 4.26 us -> 0.01 us  [from_behind(): return lax.ppermute(shard, axis, pairs)]
    all_to_all x1, blocking collectives: 41.2 us -> 44 us  [time_desk(): mid_arr = lax.all_to_all(taken_in, 'ep', 0, 0)]
  transfers between devices with their start and end apart: 4 -> 4, of which waited for: 4 -> 3; matrix products, arithmetic and copies ran while one was open for 18% -> 25% of each run, Pallas kernels for 0% -> 0%
where the time goes in v1:
time: 170 us; the launch traced here: 169 us
  blocking collectives  72 us (42%)
  waiting for transfers between devices  28.5 us (17%)
  matrix products  24.8 us (15%)
  local copies, waits for them, and re-layouts  15.4 us (9%)
  between operations  14.3 us (8%)
  starting transfers between devices  9.42 us (6%)
  other arithmetic  4.91 us (3%)
    all_to_all x1, blocking collectives, time_desk(): mid_arr = lax.all_to_all(taken_in, 'ep', 0, 0)  44 us
    all_to_all x1, blocking collectives, exchange_in_pieces(): lax.all_to_all(section, axis, split_axis=0, concat_axis=0, tiled=True)  28 us
    all_to_all x1, waiting for transfers between devices, exchange_in_pieces(): lax.all_to_all(section, axis, split_axis=0, concat_axis=0, tiled=True)  21.1 us
    unnamed x32, local copies, waits for them, and re-layouts  11.7 us
    all_gather x1, waiting for transfers between devices, gather_turned(): lax.all_gather(both, axis, axis=0, tiled=True)  6.94 us
    dot_general x1, matrix products, body(): jnp.dot(pooled, mix_weight, preferred_element_type=jnp.float32)  6.38 us
    all_to_all x1, starting transfers between devices, exchange_in_pieces(): lax.all_to_all(section, axis, split_axis=0, concat_axis=0, tiled=True)  5.95 us
    dot_general x1, matrix products, body(): jnp.einsum('erd,edf->erf', arrived, up_piece, preferred_element_type=jnp....  5.42 us
  transfers between devices with their start and end apart: 4, of which 3 were waited for; matrix products, arithmetic and copies ran while one was open for 25% of the time, Pallas kernels for 0%

profile of v1, /device:TPU:24, one launch (start us, length us, event | category | flops | bytes accessed | tf_op | source)
XLA Modules:
  0.0 169.4 jit_solution(15237307475381436052)
XLA Ops:
  7.3 2.1 %pad_maximum_fusion.1 = bf16[64,6144]{1,0:T(8,128)(2,1)} fusion(bf16[64,2048]{1,0:T(8,128)(2,1)} %bitcast.138, bf16[64,2048]{1,0:T(8,128)(2,1)} %bitcast.139, bf16[64,2048]{1,0:T(8,128)(2,1)} %bitcast.140), kind=kLoop, calls=%fused_computation.22 | loop fusion | flops 2359296 | bytes 1572864 | tf_op jit(solution)/shard_map/concatenate | solution.py:31
  9.5 0.8 slice.82
  10.3 3.4 %collective-permute-start = (bf16[15,64]{0,1:T(8,128)(2,1)S(1)}, bf16[15,64]{0,1:T(8,128)(2,1)S(1)}, u32[]{:S(2)}, u32[]{:S(2)}) collective-permute-start(bf16[15,64]{0,1:T(8,128)(2,1)S(1)} %slice.82), channel_id=1, source_target_pairs={{0,16},{16,32},{32,48},{48,64},{64,80},{80,96},{96,112},{112,128},... | collective-permute-start | bytes 5768 | tf_op jit(solution)/shard_map/ppermute | solution.py:26
  13.7 0.8 copy.29
  14.8 1.2 reduce-window.6
  16.9 2.4 %convolution_convert_fusion.1 = bf16[768,2048]{1,0:T(8,128)(2,1)S(1)} fusion(bf16[256,2048]{1,0:T(8,128)(2,1)} %param.13, f32[2048]{0:T(1024)S(1)} %copy-done.3, f32[256]{0:T(256)S(1)} %add_rsqrt_fusion, s32[256]{0:T(256)S(1)} %bitcast.141, s32[256]{0:T(256)S(1)} %bitcast.144), kind=kOutput, calls=%fused_computation.8 | convolution fusion | flops 809566208 | bytes 4205568 | tf_op jit(solution)/shard_map/dot_general | solution.py:131
  20.9 6.4 %convolution_convert_fusion = bf16[2048,2048]{1,0:T(8,128)(2,1)} fusion(bf16[64,2048]{1,0:T(8,128)(2,1)S(1)} %copy-done, f32[2063,64]{0,1:T(8,128)S(1)} %maximum_convert_fusion, f32[2062,64]{0,1:T(8,128)S(1)} %slice_add_fusion.2, f32[2060,64]{0,1:T(8,128)S(1)} %slice_add_fusion.1, f32[2056,64]{0,1:T(8,128)S(1)} %slice_add_fusion, f32[64]{0:T(128)S(1)} %copy-done.5, ...), kind=kOutput, calls=%fused_computation | convolution fusion | flops 542507008 | bytes 11283456 | tf_op jit(solution)/shard_map/dot_general | solution.py:118
  28.0 0.7 fusion.46
  28.7 0.7 fusion.45
  29.4 0.7 fusion.44
  30.8 0.7 fusion.42
  32.2 0.7 fusion.40
  37.1 0.7 fusion.33
  37.8 44.0 %all_to_all.15 = bf16[16,1,48,2048]{3,2,1,0:T(8,128)(2,1)S(1)} all-to-all(bf16[16,1,48,2048]{3,2,1,0:T(8,128)(2,1)} %fusion.33), channel_id=1, replica_groups=mesh['ep'=16,'tp'=16] {'ep'}, dimensions={0} | all-to-all | bytes 6291456 | tf_op jit(solution)/shard_map/all_to_all | solution.py:16
  81.8 6.9 %all-gather.2.cloned.1.call-done = bf16[1024,6144]{1,0:T(8,128)(2,1)} async-done(((bf16[64,6144]{1,0:T(8,128)(2,1)}), bf16[1024,6144]{1,0:T(8,128)(2,1)}) %all-gather.2.cloned.1.call-update) | async-done | bytes 12582928 | tf_op jit(solution)/shard_map/all_gather | solution.py:32
  88.8 5.4 %fusion.1 = f32[768,1024]{1,0:T(8,128)S(1)} fusion(bf16[768,2048]{1,0:T(8,128)(2,1)S(1)} %bitcast.135, bf16[1024,6144]{1,0:T(8,128)(2,1)} %all-gather.2.cloned.1.call-done), kind=kOutput, calls=%fused_computation.4 | convolution fusion | flops 3221225472 | bytes 10485760 | tf_op jit(solution)/shard_map/erd,edf->erf/dot_general | solution.py:138
  94.6 3.8 %multiply_convert_fusion = bf16[768,1024]{1,0:T(8,128)(2,1)S(1)} fusion(f32[768,1024]{1,0:T(8,128)S(1)} %fusion.1, bf16[768,2048]{1,0:T(8,128)(2,1)S(1)} %bitcast.136, bf16[1024,6144]{1,0:T(8,128)(2,1)S(1)} %copy-done.7), kind=kOutput, calls=%fused_computation.10 | convolution fusion | flops 3225944064 | bytes 12058624 | tf_op jit(solution)/shard_map/erd,edf->erf/dot_general | solution.py:137
  98.4 3.6 %fusion.3 = bf16[768,2048]{1,0:T(8,128)(2,1)S(1)} fusion(bf16[768,1024]{1,0:T(8,128)(2,1)S(1)} %multiply_convert_fusion, bf16[1024,6144]{1,0:T(8,128)(2,1)S(1)} %copy-done.7), kind=kOutput, calls=%fused_computation.7 | convolution fusion | flops 3222798336 | bytes 8912896 | tf_op jit(solution)/shard_map/erf,edf->erd/dot_general | solution.py:140
  102.1 1.4 fusion.54
  103.5 28.0 %all_to_all.16 = bf16[16,1,24,2048]{3,2,1,0:T(8,128)(2,1)S(1)} all-to-all(bf16[16,1,24,2048]{3,2,1,0:T(8,128)(2,1)S(1)} %get-tuple-element.2), channel_id=1, replica_groups=mesh['ep'=16,'tp'=16] {'ep'}, dimensions={0} | all-to-all | bytes 3145728 | tf_op jit(solution)/shard_map/all_to_all | solution.py:62
  131.5 6.0 %all-to-all-start.2 = ((bf16[16,1,24,2048]{3,2,1,0:T(8,128)(2,1)}), bf16[16,1,24,2048]{3,2,1,0:T(8,128)(2,1)S(1)}, u32[]{:S(2)}, u32[]{:S(2)}) async-start(bf16[16,1,24,2048]{3,2,1,0:T(8,128)(2,1)} %get-tuple-element.3), calls=%async_computation.3 | async-start | bytes 3145728 | tf_op jit(solution)/shard_map/all_to_all | solution.py:62
  137.4 21.1 %all-to-all-done.2 = bf16[16,1,24,2048]{3,2,1,0:T(8,128)(2,1)S(1)} async-done(((bf16[16,1,24,2048]{3,2,1,0:T(8,128)(2,1)}), bf16[16,1,24,2048]{3,2,1,0:T(8,128)(2,1)S(1)}, u32[]{:S(2)}, u32[]{:S(2)}) %all-to-all-start.2) | async-done | bytes 1572896 | tf_op jit(solution)/shard_map/all_to_all | solution.py:62
  158.9 1.1 convolution_multiply_fusion.1
  160.0 2.1 %fusion.5 = bf16[256,2048]{1,0:T(8,128)(2,1)} fusion(f32[256,2048]{1,0:T(8,128)S(1)} %convolution_multiply_fusion.1, bf16[768,2048]{1,0:T(8,128)(2,1)S(1)} %bitcast.134, f32[256]{0:T(256)S(1)} %bitcast.143, s32[256]{0:T(256)S(1)} %bitcast.142), kind=kOutput, calls=%fused_computation.16 | convolution fusion | flops 807075840 | bytes 6293504 | tf_op jit(solution)/shard_map/dot_general | solution.py:147
  (55 shorter events, 10.3 us)
Async XLA Ops:
  7.2 13.7 %copy-start = (bf16[64,2048]{1,0:T(8,128)(2,1)S(1)}, bf16[64,2048]{1,0:T(8,128)(2,1)}, u32[]{:S(2)}) copy-start(bf16[64,2048]{1,0:T(8,128)(2,1)} %param.12) | copy-start | bytes 786436
  7.2 9.7 %copy-start.4 = (s32[256,2]{0,1:T(2,128)S(1)}, s32[256,2]{0,1:T(2,128)}, u32[]{:S(2)}) copy-start(s32[256,2]{0,1:T(2,128)} %param.15) | copy-start | bytes 6148
  7.2 9.4 %copy-start.1 = (bf16[256,2048]{1,0:T(8,128)(2,1)S(1)}, bf16[256,2048]{1,0:T(8,128)(2,1)}, u32[]{:S(2)}) copy-start(bf16[256,2048]{1,0:T(8,128)(2,1)} %param.13) | copy-start | bytes 3145732
  7.2 9.7 %copy-start.3 = (f32[2048]{0:T(1024)S(1)}, f32[2048]{0:T(1024)}, u32[]{:S(2)}) copy-start(f32[2048]{0:T(1024)} %param.14) | copy-start | bytes 24580
  7.2 81.5 %all-gather.2.cloned.1.call-start = ((), (), s32[]{:S(2)}) async-start(), calls=%async_computation.5 | async-start | bytes 13369344 | tf_op jit(solution)/shard_map/all_gather | solution.py:32
  9.4 153.2 %reduce-scatter.2.cloned.1.call-start = ((), (), s32[]{:S(2)}) async-start(), calls=%async_computation.4 | async-start | bytes 8912896 | tf_op jit(solution)/shard_map/reduce_scatter | solution.py:117
  10.3 9.8 %collective-permute-start = (bf16[15,64]{0,1:T(8,128)(2,1)S(1)}, bf16[15,64]{0,1:T(8,128)(2,1)S(1)}, u32[]{:S(2)}, u32[]{:S(2)}) collective-permute-start(bf16[15,64]{0,1:T(8,128)(2,1)S(1)} %slice.82), channel_id=1, source_target_pairs={{0,16},{16,32},{32,48},{48,64},{64,80},{80,96},{96,112},{112,128},... | collective-permute-start | bytes 5768 | tf_op jit(solution)/shard_map/ppermute | solution.py:26
  16.9 3.1 %copy-start.2 = (bf16[2048,64]{0,1:T(8,128)(2,1)S(1)}, bf16[2048,64]{0,1:T(8,128)(2,1)}, u32[]{:S(2)}) copy-start(bf16[2048,64]{0,1:T(8,128)(2,1)} %param.10) | copy-start | bytes 786436
  19.3 1.5 copy-start.5
  88.7 5.8 %copy-start.7 = (bf16[1024,6144]{1,0:T(8,128)(2,1)S(1)}, bf16[1024,6144]{1,0:T(8,128)(2,1)}, u32[]{:S(2)}) copy-start(bf16[1024,6144]{1,0:T(8,128)(2,1)} %all-gather.2.cloned.1.call-done) | copy-start | bytes 37748740
  103.5 34.0 %copy-start.6 = (f32[256,2]{0,1:T(2,128)S(1)}, f32[256,2]{0,1:T(2,128)}, u32[]{:S(2)}) copy-start(f32[256,2]{0,1:T(2,128)} %param.16) | copy-start | bytes 6148
  131.5 27.0 %all-to-all-start.2 = ((bf16[16,1,24,2048]{3,2,1,0:T(8,128)(2,1)}), bf16[16,1,24,2048]{3,2,1,0:T(8,128)(2,1)S(1)}, u32[]{:S(2)}, u32[]{:S(2)}) async-start(bf16[16,1,24,2048]{3,2,1,0:T(8,128)(2,1)} %get-tuple-element.3), calls=%async_computation.3 | async-start | bytes 3145728 | tf_op jit(solution)/shard_map/all_to_all | solution.py:62
Sparse Core Ops, SparseCore 0:
  10.4 78.2 all-gather.1
  91.9 70.6 reduce-scatter.1
